TPU v7x, 32 devices: a whole 2x2x4 slice. The times are simulated.
32 devices in a mesh: sp: 4 (over z), fs: 4 (over y, x), tp: 2 (over core).
Axes of the slice: x: 2, y: 2, z: 4, core: 2. Of those that a mesh axis runs over, the one named last changes fastest.
Arguments:
- tokens: bfloat16 [8, 768, 2048], P(('fs', 'tp'), 'sp'), may hold values from -6 to 6
- linear_query: bfloat16 [2048, 512], P(('sp', 'tp'), 'fs'), may hold values from -0.125 to 0.125
- linear_key: bfloat16 [2048, 512], P(('sp', 'tp'), 'fs'), may hold values from -0.125 to 0.125
- linear_decay: bfloat16 [2048, 512], P(('sp', 'tp'), 'fs'), may hold values from -0.25 to 0.25
- linear_value: bfloat16 [2048, 1024], P(('sp', 'tp'), 'fs'), may hold values from -0.125 to 0.125
- linear_gate: bfloat16 [2048, 1024], P(('sp', 'tp'), 'fs'), may hold values from -0.125 to 0.125
- decay_bias: float32 [512], P('fs'), may hold values from 2 to 5.5
- norm_gain: float32 [256], replicated, may hold values from 0.1 to 1.9
- window_query: bfloat16 [2048, 1024], P(('sp', 'tp'), 'fs'), may hold values from -0.125 to 0.125
- window_key: bfloat16 [2048, 256], P(('sp', 'tp'), 'fs'), may hold values from -0.125 to 0.125
- window_value: bfloat16 [2048, 256], P(('sp', 'tp'), 'fs'), may hold values from -0.5 to 0.5
- sink_logit: float32 [16], P('fs'), may hold values from 3 to 7
- linear_output: bfloat16 [1024, 2048], P('fs'), may hold values from -0.1875 to 0.1875
- window_output: bfloat16 [1024, 2048], P('fs'), may hold values from -0.1875 to 0.1875
Outputs:
- mixed: bfloat16 [8, 768, 2048], P(('fs', 'tp'), 'sp')
All inputs are finite; a program needn't handle non-finite values.
Results may differ from a plain program's by a relative error of at most 0.025.
Values may be sent and summed in bfloat16 or wider, within the bound.
A program may use at most 64 MiB of HBM per device.

v0:
```python
import jax
import jax.numpy as jnp
from jax import lax
from jax.sharding import PartitionSpec as P

GLA_KEY = 128
GLA_VALUE = 256
HEAD_DIM = 64
WINDOW = 128
BLOCK = 32


norm_epsilon = 1e-05
highest = lax.Precision.HIGHEST


def over_all(x, axis, dim, block):
    whole = lax.all_gather(x, axis, axis=dim, tiled=True)
    return block(whole, jnp.int32(0))


def prefix(value, axis, join, neutral, backward):
    count, mine = lax.axis_size(axis), lax.axis_index(axis)
    pieces = jax.tree.map(lambda part: lax.all_gather(part, axis), value)
    if backward:
        pieces = jax.tree.map(lambda part: part[::-1], pieces)
        mine = count - 1 - mine
    so_far = jax.tree.map(
        lambda part, zero: jnp.full_like(part, 0) + jnp.asarray(zero, part.dtype), value, neutral
    )

    def step(position, so_far):
        longer = join(so_far, jax.tree.map(lambda part: part[position], pieces))
        return jax.tree.map(lambda new, old: jnp.where(position < mine, new, old), longer, so_far)

    return lax.fori_loop(0, count - 1, step, so_far)


def for_sending(x):
    return jax.tree.map(lambda a: a.astype(jnp.bfloat16) if a.dtype == jnp.float32 else a, x)


def shifted(x, axis, by):
    peers = lax.axis_size(axis)
    pairs = [(i, i + by) for i in range(peers) if 0 <= i + by < peers]
    return lax.ppermute(x, axis, pairs)


def own_rows(term, width, axis):
    whole = term(jnp.int32(0), width * lax.axis_size(axis)).astype(jnp.bfloat16)
    return lax.psum_scatter(whole, axis, scatter_dimension=0, tiled=True).astype(jnp.float32)


def forget_blocks(queries, key_rows, value_rows, forget_logs, block_len):
    batch_size, length, head_count, key_dim = queries.shape
    value_dim = value_rows.shape[-1]
    block_count = length // block_len

    def to_blocks(tensor):
        return tensor.reshape(
            batch_size, block_count, block_len, head_count, tensor.shape[-1]
        ).transpose(1, 0, 3, 2, 4)

    def from_blocks(tensor):
        return tensor.transpose(1, 0, 3, 2, 4).reshape(
            batch_size, length, head_count, tensor.shape[-1]
        )

    causal = jnp.tril(jnp.ones((block_len, block_len), dtype=bool))

    def advance(carry, block_inputs):
        carry_state, offset = carry
        query_blk, key_blk, value_blk, forget_blk = block_inputs
        within = jnp.cumsum(forget_blk, axis=2)
        carried = jnp.einsum(
            "bhcd,bhde->bhce", query_blk * jnp.exp(within), carry_state, precision=highest
        )
        spread = within[:, :, :, None, :] - within[:, :, None, :, :]
        decays = jnp.exp(jnp.where(causal[:, :, None], spread, -jnp.inf))
        scores = jnp.einsum(
            "bhijd,bhjd->bhij", query_blk[:, :, :, None, :] * decays, key_blk, precision=highest
        )
        inside = jnp.einsum("bhij,bhje->bhie", scores, value_blk, precision=highest)
        final_log = within[:, :, -1, :]
        faded = key_blk * jnp.exp(final_log[:, :, None, :] - within)
        new_state = carry_state * jnp.exp(final_log)[:, :, :, None] + jnp.einsum(
            "bhcd,bhce->bhde", faded, value_blk, precision=highest
        )
        reaching = jnp.exp(offset[:, :, None, :] + within)
        return ((new_state, offset + final_log), (carried + inside, reaching))

    zero_state = jnp.zeros((batch_size, head_count, key_dim, value_dim), jnp.float32)
    zero_offset = jnp.zeros((batch_size, head_count, key_dim), jnp.float32)
    blocked = (
        to_blocks(queries),
        to_blocks(key_rows),
        to_blocks(value_rows),
        to_blocks(forget_logs),
    )
    finals, produced = lax.scan(advance, (zero_state, zero_offset), blocked)
    return (from_blocks(produced[0]), from_blocks(produced[1]), finals[0], finals[1])


def finish_linear(state_rows, gate_rows, norm_gain):
    scaled = state_rows * lax.rsqrt(
        jnp.mean(jnp.square(state_rows), axis=-1, keepdims=True) + norm_epsilon
    )
    gated = scaled * norm_gain.astype(jnp.float32) * jax.nn.silu(gate_rows.astype(jnp.float32))
    return gated.reshape(state_rows.shape[0], state_rows.shape[1], -1).astype(jnp.bfloat16)


def window_attend(queries, key_rows, value_rows, sink_logit, query_first, window_len, block_len):
    batch_size, length, query_heads, head_dim = queries.shape
    prior_rows = key_rows.shape[1] - length
    kv_heads = key_rows.shape[2]
    group_size = query_heads // kv_heads
    block_count = length // block_len
    span_len = window_len + block_len
    grouped = queries.reshape(batch_size, block_count, block_len, kv_heads, group_size, head_dim)
    sink_grid = sink_logit.astype(jnp.float32).reshape(kv_heads, group_size)[None, :, :, None, None]

    def attend(block_number):
        query_blk = lax.dynamic_index_in_dim(grouped, block_number, 1, keepdims=False)
        start_row = block_number * block_len + prior_rows - window_len
        key_blk = lax.dynamic_slice_in_dim(key_rows, start_row, span_len, 1)
        value_blk = lax.dynamic_slice_in_dim(value_rows, start_row, span_len, 1)
        scores = jnp.einsum(
            "bqhgd,bkhd->bhgqk", query_blk, key_blk, precision=highest
        ) * head_dim ** (-0.5)
        query_pos = query_first + block_number * block_len + jnp.arange(block_len, dtype=jnp.int32)
        key_pos = query_first - prior_rows + start_row + jnp.arange(span_len, dtype=jnp.int32)
        distance = query_pos[:, None] - key_pos[None, :]
        allowed = (distance >= 0) & (distance < window_len) & (key_pos[None, :] >= 0)
        scores = jnp.where(allowed, scores, -jnp.inf)
        highest_score = jnp.maximum(jnp.max(scores, axis=-1, keepdims=True), sink_grid)
        weights = jnp.exp(scores - highest_score)
        normaliser = jnp.sum(weights, axis=-1, keepdims=True) + jnp.exp(sink_grid - highest_score)
        return jnp.einsum("bhgqk,bkhd->bqhgd", weights / normaliser, value_blk, precision=highest)

    blocks_out = lax.map(attend, jnp.arange(block_count, dtype=jnp.int32))
    return blocks_out.transpose(1, 0, 2, 3, 4, 5).reshape(
        batch_size, length, query_heads * head_dim
    )


def combine_states(earlier, later):
    return (earlier[0] * later[0], earlier[1] * later[0][:, :, :, None] + later[1])


def shards(
    tokens,
    linear_query,
    linear_key,
    linear_decay,
    linear_value,
    linear_gate,
    decay_bias,
    norm_gain,
    window_query,
    window_key,
    window_value,
    sink_logit,
    linear_output,
    window_output,
):
    gathered = (
        lax.all_gather(linear_query, ("sp", "tp"), axis=0, tiled=True),
        lax.all_gather(linear_key, ("sp", "tp"), axis=0, tiled=True),
        lax.all_gather(linear_decay, ("sp", "tp"), axis=0, tiled=True),
        lax.all_gather(linear_value, ("sp", "tp"), axis=0, tiled=True),
        lax.all_gather(linear_gate, ("sp", "tp"), axis=0, tiled=True),
        lax.all_gather(window_query, ("sp", "tp"), axis=0, tiled=True),
        lax.all_gather(window_key, ("sp", "tp"), axis=0, tiled=True),
        lax.all_gather(window_value, ("sp", "tp"), axis=0, tiled=True),
    )

    def project_rows(portion, first_row):
        flat_rows = portion.reshape(-1, portion.shape[-1])
        pieces = [
            jnp.dot(flat_rows, matrix, preferred_element_type=jnp.float32).astype(jnp.bfloat16)
            for matrix in gathered
        ]
        return jnp.concatenate(pieces, axis=1).reshape(portion.shape[0], portion.shape[1], -1)

    projected = over_all(tokens, "fs", 0, project_rows)
    sequences, length = (projected.shape[0], projected.shape[1])
    split_points = []
    running = 0
    for matrix in gathered[:-1]:
        running = running + matrix.shape[1]
        split_points.append(running)
    pieces_out = jnp.split(projected, split_points, axis=2)
    state_query, state_key, decay_input, state_value, state_gate = (
        pieces_out[0],
        pieces_out[1],
        pieces_out[2],
        pieces_out[3],
        pieces_out[4],
    )
    local_query, local_key, local_value = (pieces_out[5], pieces_out[6], pieces_out[7])
    state_heads = state_query.shape[2] // GLA_KEY
    tau_value = lax.axis_size("sp") * length // 16

    def linear_mixer():
        queries = state_query.astype(jnp.float32).reshape(
            sequences, length, state_heads, GLA_KEY
        ) * GLA_KEY ** (-0.5)
        key_rows = state_key.astype(jnp.float32).reshape(sequences, length, state_heads, GLA_KEY)
        value_rows = state_value.astype(jnp.float32).reshape(
            sequences, length, state_heads, GLA_VALUE
        )
        decay_rows = decay_input.astype(jnp.float32).reshape(
            sequences, length, state_heads, GLA_KEY
        )
        forget_logs = (
            jax.nn.log_sigmoid(
                decay_rows + decay_bias.astype(jnp.float32).reshape(state_heads, GLA_KEY)
            )
            / tau_value
        )
        outputs, reaching, final_state, total_log = forget_blocks(
            queries, key_rows, value_rows, forget_logs, BLOCK
        )
        decay_total = jnp.exp(total_log)
        entering = tuple(
            (
                part.astype(kind)
                for part, kind in zip(
                    prefix(
                        (decay_total.astype(jnp.bfloat16), final_state.astype(jnp.bfloat16)),
                        "sp",
                        combine_states,
                        (jnp.ones_like(decay_total), jnp.zeros_like(final_state)),
                        False,
                    ),
                    (jnp.float32, jnp.float32),
                )
            )
        )
        outputs = outputs + jnp.einsum(
            "blhd,bhde->blhe", queries * reaching, entering[1], precision=highest
        )
        gate_rows = state_gate.reshape(sequences, length, state_heads, GLA_VALUE)
        return finish_linear(outputs, gate_rows, norm_gain)

    def window_mixer():
        kv_width = local_key.shape[2]
        window_heads = kv_width // HEAD_DIM
        tail_rows = min(length, WINDOW)
        hop_count = (WINDOW + tail_rows - 1) // tail_rows
        both_rows = jnp.concatenate([local_key, local_value], axis=2)
        received = both_rows[:, length - tail_rows :]
        context = [both_rows]
        for hop_number in range(hop_count):
            received = shifted(for_sending(received), "sp", 1).astype(received.dtype)
            context = [received] + context
        joined_rows = jnp.concatenate(context, axis=1).astype(jnp.float32)
        total_rows = joined_rows.shape[1]
        key_rows = joined_rows[:, :, :kv_width].reshape(
            sequences, total_rows, window_heads, HEAD_DIM
        )
        value_rows = joined_rows[:, :, kv_width:].reshape(
            sequences, total_rows, window_heads, HEAD_DIM
        )
        queries = local_query.astype(jnp.float32).reshape(sequences, length, -1, HEAD_DIM)
        query_first = lax.axis_index("sp") * length
        return window_attend(
            queries, key_rows, value_rows, sink_logit, query_first, WINDOW, BLOCK
        ).astype(jnp.bfloat16)

    linear_rows = linear_mixer()
    window_rows = window_mixer()
    linear_flat = linear_rows.reshape(-1, linear_rows.shape[2])
    window_flat = window_rows.reshape(-1, window_rows.shape[2])

    def linear_term(first_row, row_count):
        rows_here = lax.dynamic_slice_in_dim(linear_flat, first_row, row_count, 0)
        return jnp.dot(rows_here, linear_output, preferred_element_type=jnp.float32)

    def window_term(first_row, row_count):
        rows_here = lax.dynamic_slice_in_dim(window_flat, first_row, row_count, 0)
        return jnp.dot(rows_here, window_output, preferred_element_type=jnp.float32)

    def joined_term(first_row, row_count):
        return linear_term(first_row, row_count) + window_term(first_row, row_count)

    mixed = own_rows(joined_term, length, "fs")
    return mixed.astype(jnp.bfloat16).reshape(1, length, mixed.shape[1])


def solution(mesh):
    return jax.shard_map(
        shards,
        mesh=mesh,
        in_specs=(
            P(("fs", "tp"), "sp", None),
            P(("sp", "tp"), "fs"),
            P(("sp", "tp"), "fs"),
            P(("sp", "tp"), "fs"),
            P(("sp", "tp"), "fs"),
            P(("sp", "tp"), "fs"),
            P("fs"),
            P(),
            P(("sp", "tp"), "fs"),
            P(("sp", "tp"), "fs"),
            P(("sp", "tp"), "fs"),
            P("fs"),
            P("fs", None),
            P("fs", None),
        ),
        out_specs=P(("fs", "tp"), "sp", None),
        check_vma=False,
    )
```

profile of v0, /device:TPU:24, one launch (start us, length us, event | category | flops | bytes accessed | tf_op | source)
XLA Modules:
  0.0 318.9 jit_solution(8415070174140099817)
XLA Ops:
  9.4 15.1 %all_gather.40 = bf16[2048,128]{1,0:T(8,128)(2,1)S(1)} all-gather(bf16[256,128]{1,0:T(8,128)(2,1)} %param.21), channel_id=1, replica_groups=mesh['sp'=4,'fs'=4,'tp'=2] {'sp','tp'}, dimensions={0}, use_global_device_ids=true | all-gather | bytes 589824 | tf_op jit(solution)/shard_map/all_gather | solution.py:167
  24.5 15.3 %all_gather.41 = bf16[2048,128]{1,0:T(8,128)(2,1)S(1)} all-gather(bf16[256,128]{1,0:T(8,128)(2,1)} %param.22), channel_id=1, replica_groups=mesh['sp'=4,'fs'=4,'tp'=2] {'sp','tp'}, dimensions={0}, use_global_device_ids=true | all-gather | bytes 589824 | tf_op jit(solution)/shard_map/all_gather | solution.py:168
  39.8 15.1 %all_gather.42 = bf16[2048,128]{1,0:T(8,128)(2,1)S(1)} all-gather(bf16[256,128]{1,0:T(8,128)(2,1)S(1)} %copy-done.10), channel_id=1, replica_groups=mesh['sp'=4,'fs'=4,'tp'=2] {'sp','tp'}, dimensions={0}, use_global_device_ids=true | all-gather | bytes 589824 | tf_op jit(solution)/shard_map/all_gather | solution.py:169
  54.9 15.8 %all_gather.46 = bf16[2048,64]{0,1:T(8,128)(2,1)} all-gather(bf16[256,64]{0,1:T(8,128)(2,1)S(1)} %copy-done.12), channel_id=1, replica_groups=mesh['sp'=4,'fs'=4,'tp'=2] {'sp','tp'}, dimensions={0}, use_global_device_ids=true | all-gather | bytes 294912 | tf_op jit(solution)/shard_map/all_gather | solution.py:173
  70.7 15.4 %all_gather.47 = bf16[2048,64]{0,1:T(8,128)(2,1)} all-gather(bf16[256,64]{0,1:T(8,128)(2,1)S(1)} %copy-done.13), channel_id=1, replica_groups=mesh['sp'=4,'fs'=4,'tp'=2] {'sp','tp'}, dimensions={0}, use_global_device_ids=true | all-gather | bytes 294912 | tf_op jit(solution)/shard_map/all_gather | solution.py:174
  86.1 3.9 %fusion.50 = bf16[768,1280]{0,1:T(8,128)(2,1)} fusion(bf16[768,2048]{1,0:T(8,128)(2,1)} %bitcast.246, bf16[2048,128]{1,0:T(8,128)(2,1)S(1)} %all_gather.40), kind=kOutput, calls=%fused_computation.84 | convolution fusion | flops 402751488 | bytes 3866624 | tf_op jit(solution)/shard_map/dot_general | solution.py:180
  90.0 1.9 fusion.49
  91.8 1.9 fusion.48
  93.7 3.9 %fusion.47 = bf16[768,1280]{0,1:T(8,128)(2,1)} fusion(bf16[768,1280]{0,1:T(8,128)(2,1)} %fusion.48, bf16[768,2048]{1,0:T(8,128)(2,1)} %bitcast.247, bf16[2048,256]{1,0:T(8,128)(2,1)} %all-gather.10.cloned.1.call-done), kind=kOutput, calls=%fused_computation.77 | convolution fusion | flops 805502976 | bytes 4587520 | tf_op jit(solution)/shard_map/dot_general | solution.py:180
  97.6 3.3 %all-gather.12.cloned.1.call-done = bf16[2048,256]{1,0:T(8,128)(2,1)} async-done(((bf16[256,256]{1,0:T(8,128)(2,1)}), bf16[2048,256]{1,0:T(8,128)(2,1)}) %all-gather.12.cloned.1.call-update) | async-done | bytes 1048592 | tf_op jit(solution)/shard_map/all_gather | solution.py:171
  101.0 3.9 %fusion.46 = bf16[768,1280]{0,1:T(8,128)(2,1)} fusion(bf16[768,1280]{0,1:T(8,128)(2,1)} %fusion.47, bf16[768,2048]{1,0:T(8,128)(2,1)} %bitcast.248, bf16[2048,256]{1,0:T(8,128)(2,1)} %all-gather.12.cloned.1.call-done), kind=kOutput, calls=%fused_computation.75 | convolution fusion | flops 805502976 | bytes 4587520 | tf_op jit(solution)/shard_map/dot_general | solution.py:180
  104.9 19.7 %all-gather.14.cloned.1.call-done = bf16[2048,256]{1,0:T(8,128)(2,1)} async-done(((bf16[256,256]{1,0:T(8,128)(2,1)}), bf16[2048,256]{1,0:T(8,128)(2,1)}) %all-gather.14.cloned.1.call-update) | async-done | bytes 1048592 | tf_op jit(solution)/shard_map/all_gather | solution.py:172
  124.6 4.1 %fusion.45 = bf16[768,1280]{0,1:T(8,128)(2,1)} fusion(bf16[768,1280]{0,1:T(8,128)(2,1)} %fusion.46, bf16[768,2048]{1,0:T(8,128)(2,1)} %bitcast.249, bf16[2048,256]{1,0:T(8,128)(2,1)} %all-gather.14.cloned.1.call-done), kind=kOutput, calls=%fused_computation.73 | convolution fusion | flops 805502976 | bytes 4587520 | tf_op jit(solution)/shard_map/dot_general | solution.py:180
  128.7 1.7 fusion.52
  130.4 1.7 fusion.51
  132.2 4.0 %copy.61 = bf16[768,1280]{1,0:T(8,128)(2,1)} copy(bf16[768,1280]{0,1:T(8,128)(2,1)} %fusion.51) | data formatting | bytes 3932160 | tf_op jit(solution)/shard_map/concatenate | solution.py:183
  136.2 1.8 fusion.65
  137.9 1.6 slice.19
  139.5 1.2 slice_convert_fusion
  140.7 1.5 collective-permute-start
  142.2 1.8 reshape.293
  144.1 2.1 convert_multiply_fusion.1
  146.3 50.6 %while.47 = (s32[]{:T(128)}, f32[4,1,128,256]{3,2,0,1:T(8,128)S(1)}, f32[4,1,128]{2,0,1:T(4,128)S(1)}, f32[6,4,1,32,256]{4,3,1,2,0:T(8,128)}, f32[6,4,1,32,128]{...) while((s32[]{:T(128)}, ...), condition=%wide.region_2.3_spmd.clone, body=%wide.region_0.2_spmd.clone.sunk | while | flops 122243072 | bytes 7645841 | solution.py:100
  148.4 4.2 %fusion.121 = f32[4,32,1,32]{3,2,1,0:T(1,128)S(1)} fusion(f32[4,32,128,1]{2,3,1,0:T(1,128)S(1)} %bitcast.262, f32[4,32,32,128]{3,2,1,0:T(8,128)S(1)} %exponential_multiply_fusion.2), kind=kOutput, calls=%fused_computation.29.clone.1 | convolution fusion | flops 6291456 | bytes 2179072 | tf_op jit(solution)/shard_map/while/body/eval_jaxpr/bhijd,bhjd->bhij/dot_general | solution.py:80
  152.9 1.1 fusion.123
  156.8 4.2 %fusion.121 = f32[4,32,1,32]{3,2,1,0:T(1,128)S(1)} fusion(f32[4,32,128,1]{2,3,1,0:T(1,128)S(1)} %bitcast.262, f32[4,32,32,128]{3,2,1,0:T(8,128)S(1)} %exponential_multiply_fusion.2), kind=kOutput, calls=%fused_computation.29.clone.1 | convolution fusion | flops 6291456 | bytes 2179072 | tf_op jit(solution)/shard_map/while/body/eval_jaxpr/bhijd,bhjd->bhij/dot_general | solution.py:80
  165.2 4.2 %fusion.121 = f32[4,32,1,32]{3,2,1,0:T(1,128)S(1)} fusion(f32[4,32,128,1]{2,3,1,0:T(1,128)S(1)} %bitcast.262, f32[4,32,32,128]{3,2,1,0:T(8,128)S(1)} %exponential_multiply_fusion.2), kind=kOutput, calls=%fused_computation.29.clone.1 | convolution fusion | flops 6291456 | bytes 2179072 | tf_op jit(solution)/shard_map/while/body/eval_jaxpr/bhijd,bhjd->bhij/dot_general | solution.py:80
  173.6 4.2 %fusion.121 = f32[4,32,1,32]{3,2,1,0:T(1,128)S(1)} fusion(f32[4,32,128,1]{2,3,1,0:T(1,128)S(1)} %bitcast.262, f32[4,32,32,128]{3,2,1,0:T(8,128)S(1)} %exponential_multiply_fusion.2), kind=kOutput, calls=%fused_computation.29.clone.1 | convolution fusion | flops 6291456 | bytes 2179072 | tf_op jit(solution)/shard_map/while/body/eval_jaxpr/bhijd,bhjd->bhij/dot_general | solution.py:80
  182.1 4.2 %fusion.121 = f32[4,32,1,32]{3,2,1,0:T(1,128)S(1)} fusion(f32[4,32,128,1]{2,3,1,0:T(1,128)S(1)} %bitcast.262, f32[4,32,32,128]{3,2,1,0:T(8,128)S(1)} %exponential_multiply_fusion.2), kind=kOutput, calls=%fused_computation.29.clone.1 | convolution fusion | flops 6291456 | bytes 2179072 | tf_op jit(solution)/shard_map/while/body/eval_jaxpr/bhijd,bhjd->bhij/dot_general | solution.py:80
  190.5 4.2 %fusion.121 = f32[4,32,1,32]{3,2,1,0:T(1,128)S(1)} fusion(f32[4,32,128,1]{2,3,1,0:T(1,128)S(1)} %bitcast.262, f32[4,32,32,128]{3,2,1,0:T(8,128)S(1)} %exponential_multiply_fusion.2), kind=kOutput, calls=%fused_computation.29.clone.1 | convolution fusion | flops 6291456 | bytes 2179072 | tf_op jit(solution)/shard_map/while/body/eval_jaxpr/bhijd,bhjd->bhij/dot_general | solution.py:80
  197.7 14.4 %all-gather = bf16[16,1,128]{2,1,0:T(2,128)(2,1)S(1)} all-gather(bf16[4,1,128]{2,1,0:T(2,128)(2,1)S(1)} %copy.67), channel_id=2, replica_groups=mesh['sp'=4,'fs'=4,'tp'=2] {'sp'}, dimensions={0}, use_global_device_ids=true | all-gather | bytes 5120 | tf_op jit(solution)/shard_map/all_gather | solution.py:24
  212.1 1.2 copy.66
  215.8 38.9 %while.46 = (s32[]{:T(128)}, bf16[6,4,32,1,4,64]{5,2,4,1,3,0:T(8,128)(2,1)}, s32[6]{0:T(128)S(1)}, f32[4,320,1,64]{1,3,0,2:T(8,128)}, s32[]{:T(128)}, /*index=5*...) while((s32[]{:T(128)}, ...), condition=%wide.region_9.10_spmd, body=%wide.region_6.9_spmd.sunk | while | flops 126429704 | bytes 3849869 | solution.py:140
  220.9 1.4 fusion.112
  227.4 1.4 fusion.112
  233.9 1.4 fusion.112
  240.3 1.4 fusion.112
  246.8 1.4 fusion.112
  253.3 1.4 fusion.112
  254.7 1.5 copy.75
  256.8 3.6 %while.48 = (s32[]{:T(128)}, bf16[4,1,128,256]{3,2,1,0:T(8,128)(2,1)S(1)}, s32[]{:T(128)}, bf16[4,4,1,128]{3,1,2,0:T(4,128)(2,1)S(1)}, bf16[4,4,1,128,256]{4,3,1,2,0:T(8,128)(2,1)}, /*index=5*/s32[]{:T(128)}, s32[]{:T(128)}) while((s32[]{:T(128)}, bf16[4,1,128,256]{3,2,1,0:T(8,128)(2,1)S(1)}, s32[]{:T(128)}, ...), condition=%wide.region_4.5_spmd.clone, body=%wide.region_3.4_spmd.clone.sunk | while | flops 524292 | bytes 789609 | solution.py:36
  256.8 1.2 fusion.124
  258.0 1.1 fusion.124
  259.2 1.1 fusion.124
  260.4 1.5 multiply_reduce_fusion
  262.0 1.3 fusion.58
  264.5 2.6 add_convert_fusion
  267.1 44.9 %reduce-scatter.2.cloned.1.call-done = bf16[192,2048]{1,0:T(8,128)(2,1)} async-done(((bf16[768,2048]{1,0:T(8,128)(2,1)}), bf16[192,2048]{1,0:T(8,128)(2,1)}) %reduce-scatter.2.cloned.1.call-update) | async-done | bytes 786448 | tf_op jit(solution)/shard_map/reduce_scatter | solution.py:51
  (212 shorter events, 48.9 us)
Async XLA Ops:
  6.5 256.7 %copy-start = (bf16[256,2048]{1,0:T(8,128)(2,1)S(1)}, bf16[256,2048]{1,0:T(8,128)(2,1)}, u32[]{:S(2)}) copy-start(bf16[256,2048]{1,0:T(8,128)(2,1)} %param.32) | copy-start | bytes 3145732
  6.5 33.3 %copy-start.10 = (bf16[256,128]{1,0:T(8,128)(2,1)S(1)}, bf16[256,128]{1,0:T(8,128)(2,1)}, u32[]{:S(2)}) copy-start(bf16[256,128]{1,0:T(8,128)(2,1)} %param.23) | copy-start | bytes 196612
  6.5 48.3 %copy-start.12 = (bf16[256,64]{0,1:T(8,128)(2,1)S(1)}, bf16[256,64]{0,1:T(8,128)(2,1)}, u32[]{:S(2)}) copy-start(bf16[256,64]{0,1:T(8,128)(2,1)} %param.29) | copy-start | bytes 98308
  6.5 64.1 %copy-start.13 = (bf16[256,64]{0,1:T(8,128)(2,1)S(1)}, bf16[256,64]{0,1:T(8,128)(2,1)}, u32[]{:S(2)}) copy-start(bf16[256,64]{0,1:T(8,128)(2,1)} %param.30) | copy-start | bytes 98308
  6.5 79.5 %all-gather.8.cloned.1.call-start = ((), (), s32[]{:S(2)}) async-start(), calls=%async_computation.1 | async-start | bytes 3932160 | tf_op jit(solution)/shard_map/all_gather | solution.py:18
  7.3 86.4 %all-gather.10.cloned.1.call-start = ((), (), s32[]{:S(2)}) async-start(), calls=%async_computation.2 | async-start | bytes 1179648 | tf_op jit(solution)/shard_map/all_gather | solution.py:170
  8.0 92.9 %all-gather.12.cloned.1.call-start = ((), (), s32[]{:S(2)}) async-start(), calls=%async_computation.3 | async-start | bytes 1179648 | tf_op jit(solution)/shard_map/all_gather | solution.py:171
  8.8 115.9 %all-gather.14.cloned.1.call-start = ((), (), s32[]{:S(2)}) async-start(), calls=%async_computation.4 | async-start | bytes 1179648 | tf_op jit(solution)/shard_map/all_gather | solution.py:172
  9.3 247.4 %all-gather.16.cloned.1.call-start = ((), (), s32[]{:S(2)}) async-start(), calls=%async_computation.6 | async-start | bytes 1310720 | tf_op jit(solution)/shard_map/all_gather | solution.py:24
  86.1 3.9 %copy-start.1 = (bf16[4,192,2048]{2,1,0:T(8,128)(2,1)S(1)}, bf16[4,192,2048]{2,1,0:T(8,128)(2,1)}, u32[]{:S(2)}) copy-start(bf16[4,192,2048]{2,1,0:T(8,128)(2,1)} %all-gather.8.cloned.1.call-done) | copy-start | bytes 9437188
  104.9 23.8 %copy-start.3 = (bf16[2048,64]{0,1:T(8,128)(2,1)S(1)}, bf16[2048,64]{0,1:T(8,128)(2,1)}, u32[]{:S(2)}) copy-start(bf16[2048,64]{0,1:T(8,128)(2,1)} %all_gather.46) | copy-start | bytes 786436
  124.6 4.1 %copy-start.2 = (bf16[4,192,2048]{2,1,0:T(8,128)(2,1)S(1)}, bf16[4,192,2048]{2,1,0:T(8,128)(2,1)}, u32[]{:S(2)}) copy-start(bf16[4,192,2048]{2,1,0:T(8,128)(2,1)} %all-gather.8.cloned.1.call-done) | copy-start | bytes 9437188
  128.7 1.7 copy-start.4
  140.7 3.4 %copy-start.15 = (f32[128]{0:T(128)S(1)}, f32[128]{0:T(128)}, u32[]{:S(2)}) copy-start(f32[128]{0:T(128)} %param.26) | copy-start | bytes 1540
  140.7 72.6 %collective-permute-start = (bf16[4,128,128]{2,1,0:T(8,128)(2,1)}, bf16[4,128,128]{2,1,0:T(8,128)(2,1)}, u32[]{:S(2)}, u32[]{:S(2)}) collective-permute-start(bf16[4,128,128]{2,1,0:T(8,128)(2,1)} %slice.19), channel_id=1, source_target_pairs={{0,8},{8,16},{16,24},{1,9},{9,17},{17,25},{2,10},{10,18},{18,26},{... | collective-permute-start | bytes 393224 | tf_op jit(solution)/shard_map/ppermute | solution.py:46
  144.0 2.2 copy-start.6
  196.8 16.5 %copy-start.7 = (bf16[4,192,128]{2,1,0:T(8,128)(2,1)S(1)}, bf16[4,192,128]{2,1,0:T(8,128)(2,1)}, u32[]{:S(2)}) copy-start(bf16[4,192,128]{2,1,0:T(8,128)(2,1)} %get-tuple-element.548) | copy-start | bytes 589828
  197.6 114.4 %reduce-scatter.2.cloned.1.call-start = ((), (), s32[]{:S(2)}) async-start(), calls=%async_computation.5 | async-start | bytes 3932160 | tf_op jit(solution)/shard_map/reduce_scatter | solution.py:51
  214.3 1.5 copy-start.11
  215.8 5.1 %copy-start.9 = (f32[4,320,1,64]{1,3,0,2:T(8,128)S(1)}, f32[4,320,1,64]{1,3,0,2:T(8,128)}, u32[]{:S(2)}) copy-start(f32[4,320,1,64]{1,3,0,2:T(8,128)} %get-tuple-element.797) | copy-start | bytes 983044 | tf_op jit(solution)/shard_map/while
  222.3 5.1 %copy-start.9 = (f32[4,320,1,64]{1,3,0,2:T(8,128)S(1)}, f32[4,320,1,64]{1,3,0,2:T(8,128)}, u32[]{:S(2)}) copy-start(f32[4,320,1,64]{1,3,0,2:T(8,128)} %get-tuple-element.797) | copy-start | bytes 983044 | tf_op jit(solution)/shard_map/while
  228.8 5.1 %copy-start.9 = (f32[4,320,1,64]{1,3,0,2:T(8,128)S(1)}, f32[4,320,1,64]{1,3,0,2:T(8,128)}, u32[]{:S(2)}) copy-start(f32[4,320,1,64]{1,3,0,2:T(8,128)} %get-tuple-element.797) | copy-start | bytes 983044 | tf_op jit(solution)/shard_map/while
  235.3 5.1 %copy-start.9 = (f32[4,320,1,64]{1,3,0,2:T(8,128)S(1)}, f32[4,320,1,64]{1,3,0,2:T(8,128)}, u32[]{:S(2)}) copy-start(f32[4,320,1,64]{1,3,0,2:T(8,128)} %get-tuple-element.797) | copy-start | bytes 983044 | tf_op jit(solution)/shard_map/while
  241.8 5.1 %copy-start.9 = (f32[4,320,1,64]{1,3,0,2:T(8,128)S(1)}, f32[4,320,1,64]{1,3,0,2:T(8,128)}, u32[]{:S(2)}) copy-start(f32[4,320,1,64]{1,3,0,2:T(8,128)} %get-tuple-element.797) | copy-start | bytes 983044 | tf_op jit(solution)/shard_map/while
  248.2 5.1 %copy-start.9 = (f32[4,320,1,64]{1,3,0,2:T(8,128)S(1)}, f32[4,320,1,64]{1,3,0,2:T(8,128)}, u32[]{:S(2)}) copy-start(f32[4,320,1,64]{1,3,0,2:T(8,128)} %get-tuple-element.797) | copy-start | bytes 983044 | tf_op jit(solution)/shard_map/while
  256.8 3.6 %copy-start.8 = (f32[6,4,1,32,128]{4,3,0,1,2:T(8,128)S(1)}, f32[6,4,1,32,128]{4,3,0,1,2:T(8,128)}, u32[]{:S(2)}) copy-start(f32[6,4,1,32,128]{4,3,0,1,2:T(8,128)} %get-tuple-element.355) | copy-start | bytes 1179652
  260.4 1.6 copy-start.14
  263.3 1.2 copy-start.5
Sparse Core Ops, SparseCore 0:
  9.2 44.6 all-gather.7
  55.4 21.5 all-gather.9
  78.6 22.2 all-gather.11
  102.4 22.1 all-gather.13
  197.7 28.5 all-gather.15
  267.3 44.7 reduce-scatter.1
where the time goes:
time: 322 us; the launch traced here: 319 us
  blocking collectives  91.1 us (28%)
  matrix products  79 us (25%)
  waiting for transfers between devices  70.5 us (22%)
  local copies, waits for them, and re-layouts  28.6 us (9%)
  other arithmetic  20.3 us (6%)
  loops' own time  13.9 us (4%)
  between operations  13.7 us (4%)
    reduce_scatter x1, waiting for transfers between devices, own_rows(): lax.psum_scatter(whole, axis, scatter_dimension=0, tiled=True)  44.9 us
    dot_general x6, matrix products, advance(): jnp.einsum('bhijd,bhjd->bhij', query_blk[:, :, :, None, :] * decays, key_...  25.2 us
    dot_general x8, matrix products, project_rows(): jnp.dot(flat_rows, matrix, preferred_element_type=jnp.float32)  23 us
    all_gather x1, waiting for transfers between devices, shards(): lax.all_gather(window_query, ('sp', 'tp'), axis=0, tiled=True)  19.7 us
    all_gather x1, blocking collectives, shards(): lax.all_gather(window_key, ('sp', 'tp'), axis=0, tiled=True)  15.8 us
    all_gather x1, blocking collectives, shards(): lax.all_gather(window_value, ('sp', 'tp'), axis=0, tiled=True)  15.4 us
    all_gather x1, blocking collectives, shards(): lax.all_gather(linear_key, ('sp', 'tp'), axis=0, tiled=True)  15.3 us
    all_gather x1, blocking collectives, shards(): lax.all_gather(linear_query, ('sp', 'tp'), axis=0, tiled=True)  15.1 us
  transfers between devices with their start and end apart: 7, of which 3 were waited for; matrix products, arithmetic and copies ran while one was open for 32% of the time, Pallas kernels for 0%

commit v1 on v0

v1 whole, which is shorter than its diff:
```python
import functools

import jax
import jax.numpy as jnp
from jax import lax
from jax.experimental import pallas as pl
from jax.experimental.pallas import tpu as pltpu
from jax.sharding import PartitionSpec as P

GLA_KEY = 128
GLA_VALUE = 256
HEAD_DIM = 64
WINDOW = 128

norm_epsilon = 1e-05
MESH = pl.DeviceIdType.MESH
f32, bf16 = jnp.float32, jnp.bfloat16


def dot(a, b):
    return jnp.dot(a, b, preferred_element_type=f32)


def dot_t(a, b):
    return lax.dot_general(a, b, (((1,), (1,)), ((), ())), preferred_element_type=f32)


def dot_rows(a, b):
    return lax.dot_general(a, b, (((0,), (0,)), ((), ())), preferred_element_type=f32)


def kernel(
    NZ, NF, NT, levels,
    tok, w1, w2, w3, bias, gain, sink, out_w,
    out,
    toks, W1, W2, W3, sums, fhi, flo, kkey, val, kvbuf, qs, oacc, state_in, state_out,
    rows, part, rbuf,
    loc_sem, wsend, wrecv, fsend, frecv, tsend, trecv, ssend, srecv, hsend, hrecv, psend, precv,
):
    z, f, t = lax.axis_index("sp"), lax.axis_index("fs"), lax.axis_index("tp")
    length = tok.shape[0]
    tau = NZ * length // 16

    barrier = pltpu.get_barrier_semaphore()
    for d in range(1, NZ):
        pl.semaphore_signal(barrier, inc=1, device_id={"sp": lax.rem(z + d, NZ)}, device_id_type=MESH)
    for d in range(1, NF):
        pl.semaphore_signal(barrier, inc=1, device_id={"fs": lax.rem(f + d, NF)}, device_id_type=MESH)
    for d in range(1, NT):
        pl.semaphore_signal(barrier, inc=1, device_id={"tp": lax.rem(t + d, NT)}, device_id_type=MESH)
    pl.semaphore_wait(barrier, NZ + NF + NT - 3)

    own = z * NT + t
    groups = ((w1, W1), (w2, W2), (w3, W3))

    def token_copy(d):
        return pltpu.make_async_remote_copy(
            src_ref=tok, dst_ref=toks.at[f], send_sem=tsend.at[d], recv_sem=trecv.at[d],
            device_id={"fs": lax.rem(f + d, NF)}, device_id_type=MESH)

    def weight_copy(g, d):
        src, dst = groups[g]
        return pltpu.make_async_remote_copy(
            src_ref=src, dst_ref=dst.at[own], send_sem=wsend.at[g, d], recv_sem=wrecv.at[g, d],
            device_id={"sp": lax.rem(z + d, NZ)}, device_id_type=MESH)

    def forward_copy(g, d, e):
        src, dst = groups[g]
        slot = lax.rem(z - d + NZ, NZ) * NT + t
        return pltpu.make_async_remote_copy(
            src_ref=src if d == 0 else dst.at[slot], dst_ref=dst.at[slot],
            send_sem=fsend.at[g, d, e], recv_sem=frecv.at[g, d, e],
            device_id={"tp": lax.rem(t + e, NT)}, device_id_type=MESH)

    for d in range(1, NF):
        token_copy(d).start()
    for g in range(3):
        for d in range(1, NZ):
            weight_copy(g, d).start()
        for e in range(1, NT):
            forward_copy(g, 0, e).start()
    local = [pltpu.make_async_copy(tok, toks.at[f], loc_sem.at[0])]
    for g in range(3):
        local.append(pltpu.make_async_copy(groups[g][0], groups[g][1].at[own], loc_sem.at[1 + g]))
    for c in local:
        c.start()

    i = lax.broadcasted_iota(jnp.int32, (length, length), 0)
    s = lax.broadcasted_iota(jnp.int32, (length, length), 1)
    for n, h in enumerate(levels):
        ref = (i & ~(2 * h - 1)) + h - 1
        later = (i & h) != 0
        low = jnp.where(later, ref, i)
        high = jnp.where(later, i, ref)
        sums[n] = jnp.where((s > low) & (s <= high), 1.0, 0.0).astype(bf16)
    sums[len(levels)] = jnp.where(s <= i, 1.0, 0.0).astype(bf16)
    sums[len(levels) + 1] = jnp.where(s > i, 1.0, 0.0).astype(bf16)

    @pl.when(z == 0)
    def _():
        state_in[...] = jnp.zeros_like(state_in)
        kvbuf[:, 0:WINDOW, :] = jnp.zeros((NF, WINDOW, kvbuf.shape[2]), bf16)

    for c in local:
        c.wait()

    def arrive(g):
        for d in range(1, NZ):
            weight_copy(g, d).wait_recv()
            for e in range(1, NT):
                forward_copy(g, d, e).start()
        for d in range(NZ):
            for e in range(1, NT):
                forward_copy(g, d, e).wait_recv()

    def log_sum(n, b):
        m = sums[n]
        return dot(m, fhi[b]) + dot(m, flo[b])

    depth = tok.shape[1]
    arrive(0)
    for d in range(1, NF):
        token_copy(d).wait_recv()

    @pl.loop(0, NF)
    def _(b):
        p = dot(toks[b], W1[...].reshape(depth, -1)).astype(bf16)
        x = p[:, :GLA_KEY].astype(f32) + bias[...]
        forget = (jnp.minimum(x, 0.0) - jnp.log1p(jnp.exp(-jnp.abs(x)))) / tau
        hi = forget.astype(bf16)
        fhi[b] = hi
        flo[b] = (forget - hi.astype(f32)).astype(bf16)
        kkey[b] = p[:, GLA_KEY:2 * GLA_KEY]
        val[b] = p[:, 2 * GLA_KEY:2 * GLA_KEY + GLA_VALUE]
        kvbuf[b, WINDOW:, :] = p[:, 2 * GLA_KEY + GLA_VALUE:]

    def halo_copy():
        return pltpu.make_async_remote_copy(
            src_ref=kvbuf.at[:, pl.ds(length, WINDOW)], dst_ref=kvbuf.at[:, pl.ds(0, WINDOW)],
            send_sem=hsend, recv_sem=hrecv, device_id={"sp": lax.rem(z + 1, NZ)}, device_id_type=MESH)

    def state_copy(b):
        return pltpu.make_async_remote_copy(
            src_ref=state_out.at[b], dst_ref=state_in.at[b],
            send_sem=ssend.at[b], recv_sem=srecv.at[b],
            device_id={"sp": lax.rem(z + 1, NZ)}, device_id_type=MESH)

    @pl.when(z < NZ - 1)
    def _():
        halo_copy().start()

    @pl.loop(0, NF)
    def _(b):
        faded = (kkey[b].astype(f32) * jnp.exp(log_sum(len(levels) + 1, b))).astype(bf16)
        local_state = dot_rows(faded, val[b])
        ones = jnp.ones((length, GLA_VALUE), bf16)
        decay = jnp.exp(dot_rows(fhi[b], ones) + dot_rows(flo[b], ones))

        @pl.when(z > 0)
        def _():
            state_copy(b).wait_recv()

        @pl.when(z < NZ - 1)
        def _():
            state_out[b] = (state_in[b].astype(f32) * decay + local_state).astype(bf16)
            state_copy(b).start()

    arrive(1)

    @pl.when(z > 0)
    def _():
        halo_copy().wait_recv()

    span = length + WINDOW
    row = lax.broadcasted_iota(jnp.int32, (length, span), 0)
    col = lax.broadcasted_iota(jnp.int32, (length, span), 1)
    distance = row - col + WINDOW
    heads = sink.shape[1]
    wq = heads * HEAD_DIM

    @pl.loop(0, NF)
    def _(b):
        p = dot(toks[b], W2[...].reshape(depth, -1)).astype(bf16)
        allowed = (distance >= 0) & (distance < WINDOW) & ((col >= WINDOW) | (z > 0))
        kv = kvbuf[b]
        k, v = kv[:, :HEAD_DIM], kv[:, HEAD_DIM:]
        heads_out = []
        for j in range(heads):
            score = dot_t(p[:, j * HEAD_DIM:(j + 1) * HEAD_DIM], k) * HEAD_DIM ** -0.5
            score = jnp.where(allowed, score, -jnp.inf)
            sk = sink[0:1, j:j + 1]
            top = jnp.maximum(jnp.max(score, axis=1, keepdims=True), sk)
            e = jnp.exp(score - top)
            total = jnp.sum(e, axis=1, keepdims=True) + jnp.exp(sk - top)
            heads_out.append((dot(e.astype(bf16), v) / total).astype(bf16))
        rows[b, :, GLA_VALUE:] = jnp.concatenate(heads_out, axis=1)
        q = p[:, wq:].astype(f32) * GLA_KEY ** -0.5
        k = kkey[b].astype(f32)
        v = val[b]
        ri = lax.broadcasted_iota(jnp.int32, (length, length), 0)
        ci = lax.broadcasted_iota(jnp.int32, (length, length), 1)
        rk = lax.broadcasted_iota(jnp.int32, (length, GLA_KEY), 0)
        scores = jnp.where(ri == ci, dot_t(q.astype(bf16), kkey[b]), 0.0)
        for n, h in enumerate(levels):
            decay = jnp.exp(log_sum(n, b))
            later = (rk & h) != 0
            qh = jnp.where(later, q * decay, 0.0).astype(bf16)
            kh = jnp.where(later, 0.0, k * decay).astype(bf16)
            same = (ri & ~(2 * h - 1)) == (ci & ~(2 * h - 1))
            scores = scores + jnp.where(same, dot_t(qh, kh), 0.0)
        reach = (q * jnp.exp(log_sum(len(levels), b))).astype(bf16)
        oacc[b] = dot(scores.astype(bf16), v) + dot(reach, state_in[b])

    arrive(2)

    def part_copy(d):
        return pltpu.make_async_remote_copy(
            src_ref=part.at[d], dst_ref=rbuf.at[d], send_sem=psend.at[d], recv_sem=precv.at[d],
            device_id={"fs": lax.rem(f + d, NF)}, device_id_type=MESH)

    @pl.loop(1, NF + 1)
    def _(step):
        b = lax.rem(f + step, NF)
        gate = dot(toks[b], W3[...].reshape(depth, -1)).astype(bf16).astype(f32)
        o = oacc[b]
        scaled = o * lax.rsqrt(jnp.mean(o * o, axis=1, keepdims=True) + norm_epsilon)
        rows[b, :, :GLA_VALUE] = (scaled * gain[...] * (gate / (1.0 + jnp.exp(-gate)))).astype(bf16)
        y = dot(rows[b], out_w[...])

        @pl.when(step < NF)
        def _():
            part[step] = y.astype(bf16)
            part_copy(step).start()

        @pl.when(step == NF)
        def _():
            acc = y
            for d in range(1, NF):
                part_copy(d).wait_recv()
                acc = acc + rbuf[d].astype(f32)
            out[...] = acc.astype(bf16)

    for d in range(1, NF):
        token_copy(d).wait_send()
        part_copy(d).wait_send()
    for g in range(3):
        for d in range(1, NZ):
            weight_copy(g, d).wait_send()
        for d in range(NZ):
            for e in range(1, NT):
                forward_copy(g, d, e).wait_send()

    @pl.when(z < NZ - 1)
    def _():
        halo_copy().wait_send()
        for b in range(NF):
            state_copy(b).wait_send()


def shards(
    NZ, NF, NT,
    tokens, linear_query, linear_key, linear_decay, linear_value, linear_gate, decay_bias,
    norm_gain, window_query, window_key, window_value, sink_logit, linear_output, window_output,
):
    _, length, depth = tokens.shape
    w1 = jnp.concatenate([linear_decay, linear_key, linear_value, window_key, window_value], axis=1)
    w2 = jnp.concatenate([window_query, linear_query], axis=1)
    w3 = linear_gate
    out_w = jnp.concatenate([linear_output, window_output], axis=0)
    kb = w1.shape[0]
    n = NZ * NT
    levels = []
    h = 1
    while h < length:
        levels.append(h)
        h *= 2
    vm = pltpu.VMEM
    dma = pltpu.SemaphoreType.DMA
    kv_width = window_key.shape[1] + window_value.shape[1]
    out_rows = out_w.shape[0]
    result = pl.pallas_call(
        functools.partial(kernel, NZ, NF, NT, tuple(levels)),
        out_shape=jax.ShapeDtypeStruct((length, depth), bf16),
        in_specs=[pl.BlockSpec(memory_space=vm)] * 8,
        out_specs=pl.BlockSpec(memory_space=vm),
        scratch_shapes=[
            vm((NF, length, depth), bf16),
            vm((n, kb, w1.shape[1]), bf16),
            vm((n, kb, w2.shape[1]), bf16),
            vm((n, kb, w3.shape[1]), bf16),
            vm((len(levels) + 2, length, length), bf16),
            vm((NF, length, GLA_KEY), bf16),
            vm((NF, length, GLA_KEY), bf16),
            vm((NF, length, GLA_KEY), bf16),
            vm((NF, length, GLA_VALUE), bf16),
            vm((NF, length + WINDOW, kv_width), bf16),
            vm((8, 128), f32),
            vm((NF, length, GLA_VALUE), f32),
            vm((NF, GLA_KEY, GLA_VALUE), bf16),
            vm((NF, GLA_KEY, GLA_VALUE), bf16),
            vm((NF, length, out_rows), bf16),
            vm((NF, length, depth), bf16),
            vm((NF, length, depth), bf16),
            dma((4,)),
            dma((3, NZ)), dma((3, NZ)),
            dma((3, NZ, NT)), dma((3, NZ, NT)),
            dma((NF,)), dma((NF,)),
            dma((NF,)), dma((NF,)),
            dma, dma,
            dma((NF,)), dma((NF,)),
        ],
        compiler_params=pltpu.CompilerParams(
            collective_id=0, has_side_effects=True, vmem_limit_bytes=60 * 1024 * 1024),
        name="layer",
    )(tokens[0], w1, w2, w3, decay_bias[None], norm_gain[None], sink_logit[None], out_w)
    return result[None]


def solution(mesh):
    shape = mesh.shape
    return jax.shard_map(
        functools.partial(shards, shape["sp"], shape["fs"], shape["tp"]),
        mesh=mesh,
        in_specs=(
            P(("fs", "tp"), "sp", None),
            P(("sp", "tp"), "fs"),
            P(("sp", "tp"), "fs"),
            P(("sp", "tp"), "fs"),
            P(("sp", "tp"), "fs"),
            P(("sp", "tp"), "fs"),
            P("fs"),
            P(),
            P(("sp", "tp"), "fs"),
            P(("sp", "tp"), "fs"),
            P(("sp", "tp"), "fs"),
            P("fs"),
            P("fs", None),
            P("fs", None),
        ),
        out_specs=P(("fs", "tp"), "sp", None),
        check_vma=False,
    )
```

time: 322 us -> 146 us (0.45)
  Pallas kernels: 0 us -> 134 us
  blocking collectives: 91.1 us -> 0 us
  matrix products: 79 us -> 0 us
  waiting for transfers between devices: 70.5 us -> 0 us
  local copies, waits for them, and re-layouts: 28.6 us -> 5.65 us
  other arithmetic: 20.3 us -> 4.78 us
  loops' own time: 13.9 us -> 0 us
  between operations: 13.7 us -> 0.02 us
    pallas_call x0 -> x1, Pallas kernels: none -> 134 us  [shards(): pl.pallas_call(functools.partial(kernel, NZ, NF, NT, tuple(levels)), out_...]
    all_gather x6 -> x0, blocking collectives: 91.1 us -> none  [the longest x1 15.8 us: shards(): lax.all_gather(window_key, ('sp', 'tp'), axis=0, tiled=True)]
    dot_general x47 -> x0, matrix products: 79 us -> none  [the longest x6 25.2 us: advance(): jnp.einsum('bhijd,bhjd->bhij', query_blk[:, :, :, None, :] * decays, key_...]
    reduce_scatter x1 -> x0, waiting for transfers between devices: 44.9 us -> none  [own_rows(): lax.psum_scatter(whole, axis, scatter_dimension=0, tiled=True)]
    all_gather x5 -> x0, waiting for transfers between devices: 23 us -> none  [the longest x1 19.7 us: shards(): lax.all_gather(window_query, ('sp', 'tp'), axis=0, tiled=True)]
    another operation x3 -> x0, loops' own time: 13.9 us -> none  [the longest x1 13.5 us: window_attend(): blocks_out = lax.map(attend, jnp.arange(block_count, dtype=jnp.int32))]
    dynamic_slice x12 -> x0, local copies, waits for them, and re-layouts: 9.17 us -> none  [the longest x6 5.86 us: attend(): lax.dynamic_index_in_dim(grouped, block_number, 1, keepdims=False)]
    squeeze x12 -> x0, local copies, waits for them, and re-layouts: 5.15 us -> none  [forget_blocks(): finals, produced = lax.scan(advance, (zero_state, zero_offset), blocked)]
  transfers between devices with their start and end apart: 7 -> 0, of which waited for: 3 -> 0; matrix products, arithmetic and copies ran while one was open for 32% -> 0% of each run, Pallas kernels for 0% -> 0%
where the time goes in v1:
time: 146 us; the launch traced here: 145 us
  Pallas kernels  134 us (92%)
  local copies, waits for them, and re-layouts  5.65 us (4%)
  other arithmetic  4.78 us (3%)
    pallas_call x1, Pallas kernels, shards(): pl.pallas_call(functools.partial(kernel, NZ, NF, NT, tuple(levels)), out_...  134 us
    unnamed x3, local copies, waits for them, and re-layouts  3.83 us
    concatenate x1, other arithmetic, shards(): out_w = jnp.concatenate([linear_output, window_output], axis=0)  3.14 us

profile of v1, /device:TPU:24, one launch (start us, length us, event | category | flops | bytes accessed | tf_op | source)
XLA Modules:
  0.0 144.6 jit_solution(4347956007497064420)
XLA Ops:
  0.0 0.9 copy.15
  0.9 0.9 copy.16
  1.8 1.8 %concatenate.9.w1 = bf16[256,640]{1,0:T(8,128)(2,1)} concatenate(bf16[256,128]{1,0:T(8,128)(2,1)} %param.17, bf16[256,128]{1,0:T(8,128)(2,1)} %param.16, bf16[256,256]{1,0:T(8,128)(2,1)} %param.18, bf16[256,64]{1,0:T(8,128)(2,1)S(1)} %copy.15, bf16[256,64]{1,0:T(8,128)(2,1)S(1)} %copy.16), dimensions={1} | concatenate | bytes 655360 | tf_op jit(solution)/shard_map/concatenate | solution.py:266
  3.6 1.6 %pad_maximum_fusion.1.w2 = bf16[256,384]{1,0:T(8,128)(2,1)} fusion(bf16[256,128]{1,0:T(8,128)(2,1)} %param.15, bf16[256,256]{1,0:T(8,128)(2,1)} %param.22), kind=kLoop, calls=%fused_computation.1 | loop fusion | flops 393216 | bytes 393216 | tf_op jit(solution)/shard_map/concatenate | solution.py:267
  5.2 3.1 %pad_maximum_fusion.out_w = bf16[512,2048]{1,0:T(8,128)(2,1)} fusion(bf16[256,2048]{1,0:T(8,128)(2,1)} %param.27, bf16[256,2048]{1,0:T(8,128)(2,1)} %param.26), kind=kLoop, calls=%fused_computation | loop fusion | flops 4194304 | bytes 4194304 | tf_op jit(solution)/shard_map/concatenate | solution.py:269
  8.4 134.1 %layer.1 = bf16[192,2048]{1,0:T(8,128)(2,1)} custom-call(bf16[192,2048]{1,0:T(8,128)(2,1)} %bitcast.6, bf16[256,640]{1,0:T(8,128)(2,1)} %concatenate.9.w1, bf16[256,384]{1,0:T(8,128)(2,1)} %pad_maximum_fusion.1.w2, bf16[256,256]{1,0:T(8,128)(2,1)} %w3.1, f32[1,128]{1,0:T(1,128)} %bitcast.8, f32[1,256]{1,0:T(1,128)} %bitcast.7, f32[1,4]{1,0:T(1,128)} %bitcast.9, ...), custom_call_target="tpu_custom_call" | custom-call | tf_op jit(solution)/shard_map/layer/pallas_call | solution.py:281
  142.5 2.1 %copy.18 = bf16[1,192,2048]{2,1,0:T(8,128)(2,1)} copy(bf16[1,192,2048]{2,1,0:T(8,128)(2,1)} %bitcast.5) | data formatting | bytes 1572864

commit v2 on v1

v2 whole, which is shorter than its diff:
```python
import functools

import jax
import jax.numpy as jnp
from jax import lax
from jax.experimental import pallas as pl
from jax.experimental.pallas import tpu as pltpu
from jax.sharding import PartitionSpec as P

GLA_KEY = 128
GLA_VALUE = 256
HEAD_DIM = 64
WINDOW = 128

norm_epsilon = 1e-05
MESH = pl.DeviceIdType.MESH
f32, bf16 = jnp.float32, jnp.bfloat16


def dot(a, b):
    return jnp.dot(a, b, preferred_element_type=f32)


def dot_t(a, b):
    return lax.dot_general(a, b, (((1,), (1,)), ((), ())), preferred_element_type=f32)


def dot_rows(a, b):
    return lax.dot_general(a, b, (((0,), (0,)), ((), ())), preferred_element_type=f32)


def kernel(
    NZ, NF, NT, levels, places,
    tok, decay_w, key_w, query_w, value_w, wquery_w, wkv_w, gate_w, bias, gain, sink, lin_w, win_w,
    out,
    toks, W1, W2, W3, out_w, sums, fhi, flo, kkey, val, kvbuf, qs, wqs, reach, oacc, loc_state, loc_decay,
    state_in, state_out, rows, part, rx, ry, dA, dB,
    loc_sem, wsend, wrecv, osend, orecv, fsend, frecv, tsend, trecv, ssend, srecv, hsend, hrecv, psend, precv,
):
    z, f, t = lax.axis_index("sp"), lax.axis_index("fs"), lax.axis_index("tp")
    length, depth = tok.shape[1:]
    half = length // 2
    tau = NZ * length // 16
    fx = f + 1 - 2 * lax.rem(f, 2)
    fy = lax.rem(f + 2, 4)
    fd = 3 - f

    barrier = pltpu.get_barrier_semaphore()
    for d in range(1, NZ):
        pl.semaphore_signal(barrier, inc=1, device_id={"sp": lax.rem(z + d, NZ)}, device_id_type=MESH)
    for peer in (fx, fy):
        pl.semaphore_signal(barrier, inc=1, device_id={"fs": peer}, device_id_type=MESH)
    for d in range(1, NT):
        pl.semaphore_signal(barrier, inc=1, device_id={"tp": lax.rem(t + d, NT)}, device_id_type=MESH)
    pl.semaphore_wait(barrier, NZ + NT)

    own = z * NT + t
    buffers = (W1, W2, W3)
    sources = ((decay_w, key_w, query_w, value_w), (wquery_w, wkv_w), (gate_w,))
    pieces = []
    for g in range(3):
        for src, col in zip(sources[g], places[g]):
            pieces.append((g, src, buffers[g].at[own, :, pl.ds(col, src.shape[1])]))

    top, low_half = pl.ds(0, half), pl.ds(half, half)

    def remote(src, dst, send, recv, axis, peer):
        return pltpu.make_async_remote_copy(
            src_ref=src, dst_ref=dst, send_sem=send, recv_sem=recv,
            device_id={axis: peer}, device_id_type=MESH)

    def token_copy(n):
        part_rows = (top, low_half, low_half, top)[n] if n < 4 else (top, low_half)[n - 4]
        if n < 4:
            return remote(tok.at[0, part_rows], toks.at[f, part_rows], tsend.at[n], trecv.at[n],
                          "fs", fx if n < 2 else fy)
        slot = (fx, fy)[n - 4]
        return remote(toks.at[slot, part_rows], toks.at[slot, part_rows], tsend.at[n], trecv.at[n],
                      "fs", (fy, fx)[n - 4])

    def weight_copy(n, d):
        g, src, dst = pieces[n]
        return remote(src, dst, wsend.at[n, d], wrecv.at[n, d], "sp", lax.rem(z + d, NZ))

    def own_copy(n, e):
        g, src, dst = pieces[n]
        return remote(src, dst, osend.at[n, e], orecv.at[n, e], "tp", lax.rem(t + e, NT))

    def forward_copy(g, d, e):
        block = buffers[g].at[lax.rem(z - d + NZ, NZ) * NT + t]
        return remote(block, block, fsend.at[g, d, e], frecv.at[g, d, e], "tp", lax.rem(t + e, NT))

    for n in range(4):
        token_copy(n).start()
    for n in range(len(pieces)):
        for d in range(1, NZ):
            weight_copy(n, d).start()
        for e in range(1, NT):
            own_copy(n, e).start()
    local = [
        pltpu.make_async_copy(tok.at[0], toks.at[f], loc_sem.at[0]),
        pltpu.make_async_copy(lin_w, out_w.at[pl.ds(0, lin_w.shape[0])], loc_sem.at[1]),
        pltpu.make_async_copy(win_w, out_w.at[pl.ds(lin_w.shape[0], win_w.shape[0])], loc_sem.at[2]),
    ]
    for n, (g, src, dst) in enumerate(pieces):
        local.append(pltpu.make_async_copy(src, dst, loc_sem.at[3 + n]))
    for c in local:
        c.start()

    i = lax.broadcasted_iota(jnp.int32, (length, length), 0)
    s = lax.broadcasted_iota(jnp.int32, (length, length), 1)
    for n, h in enumerate(levels):
        ref = (i & ~(2 * h - 1)) + h - 1
        later = (i & h) != 0
        low = jnp.where(later, ref, i)
        high = jnp.where(later, i, ref)
        sums[n] = jnp.where((s > low) & (s <= high), 1.0, 0.0).astype(bf16)
    sums[len(levels)] = jnp.where(s <= i, 1.0, 0.0).astype(bf16)
    sums[len(levels) + 1] = jnp.where(s > i, 1.0, 0.0).astype(bf16)

    @pl.when(z == 0)
    def _():
        state_in[...] = jnp.zeros_like(state_in)
        kvbuf[:, 0:WINDOW, :] = jnp.zeros((NF, WINDOW, kvbuf.shape[2]), bf16)

    token_copy(0).wait_recv()
    token_copy(4).start()
    token_copy(2).wait_recv()
    token_copy(5).start()
    for c in local:
        c.wait()

    def arrive(g):
        for d in range(1, NZ):
            for n, piece in enumerate(pieces):
                if piece[0] == g:
                    weight_copy(n, d).wait_recv()
            for e in range(1, NT):
                forward_copy(g, d, e).start()
        for e in range(1, NT):
            for n, piece in enumerate(pieces):
                if piece[0] == g:
                    own_copy(n, e).wait_recv()
            for d in range(1, NZ):
                forward_copy(g, d, e).wait_recv()

    def log_sum(n, b):
        m = sums[n]
        return dot(m, fhi[b]) + dot(m, flo[b])

    def project(buffer, col, width):
        x = toks[...].reshape(NF * length, depth)
        w = buffer[:, :, col:col + width].reshape(depth, width)
        return dot(x, w).astype(bf16).reshape(NF, length, width)

    for n in (1, 3, 4, 5):
        token_copy(n).wait_recv()
    arrive(0)
    pair = project(W1, 0, 2 * GLA_KEY)
    x = pair[:, :, :GLA_KEY].astype(f32) + bias[...]
    forget = (jnp.minimum(x, 0.0) - jnp.log1p(jnp.exp(-jnp.abs(x)))) / tau
    hi = forget.astype(bf16)
    fhi[...] = hi
    flo[...] = (forget - hi.astype(f32)).astype(bf16)
    kkey[...] = pair[:, :, GLA_KEY:]
    rest = project(W1, 2 * GLA_KEY, GLA_KEY + GLA_VALUE)
    qs[...] = rest[:, :, :GLA_KEY]
    val[...] = rest[:, :, GLA_KEY:]

    def halo_copy():
        return remote(kvbuf.at[:, pl.ds(length, WINDOW)], kvbuf.at[:, pl.ds(0, WINDOW)],
                      hsend, hrecv, "sp", lax.rem(z + 1, NZ))

    def state_copy(b):
        return remote(state_out.at[b], state_in.at[b], ssend.at[b], srecv.at[b],
                      "sp", lax.rem(z + 1, NZ))

    @pl.loop(0, NF)
    def _(b):
        faded = (kkey[b].astype(f32) * jnp.exp(log_sum(len(levels) + 1, b))).astype(bf16)
        state = dot_rows(faded, val[b])
        ones = jnp.ones((length, GLA_VALUE), bf16)
        loc_state[b] = state
        loc_decay[b] = jnp.exp(dot_rows(fhi[b], ones) + dot_rows(flo[b], ones))

        @pl.when(z == 0)
        def _():
            state_out[b] = state.astype(bf16)
            state_copy(b).start()

    @pl.loop(0, NF)
    def _(b):
        q = qs[b].astype(f32) * GLA_KEY ** -0.5
        k = kkey[b].astype(f32)
        ri = lax.broadcasted_iota(jnp.int32, (length, length), 0)
        ci = lax.broadcasted_iota(jnp.int32, (length, length), 1)
        rk = lax.broadcasted_iota(jnp.int32, (length, GLA_KEY), 0)
        scores = jnp.where(ri == ci, dot_t(q.astype(bf16), kkey[b]), 0.0)
        for n, h in enumerate(levels):
            decay = jnp.exp(log_sum(n, b))
            later = (rk & h) != 0
            qh = jnp.where(later, q * decay, 0.0).astype(bf16)
            kh = jnp.where(later, 0.0, k * decay).astype(bf16)
            same = (ri & ~(2 * h - 1)) == (ci & ~(2 * h - 1))
            scores = scores + jnp.where(same, dot_t(qh, kh), 0.0)
        reach[b] = (q * jnp.exp(log_sum(len(levels), b))).astype(bf16)
        oacc[b] = dot(scores.astype(bf16), val[b])

        @pl.when((z > 0) & (z < NZ - 1))
        def _():
            state_copy(b).wait_recv()
            state_out[b] = (state_in[b].astype(f32) * loc_decay[b] + loc_state[b]).astype(bf16)
            state_copy(b).start()

    arrive(1)
    heads = sink.shape[1]
    wq = heads * HEAD_DIM
    kvbuf[:, WINDOW:, :] = project(W2, wq, kvbuf.shape[2])

    @pl.when(z < NZ - 1)
    def _():
        halo_copy().start()

    wqs[...] = project(W2, 0, wq)

    @pl.when(z > 0)
    def _():
        halo_copy().wait_recv()

    span = length + WINDOW

    @pl.loop(0, NF)
    def _(b):
        row = lax.broadcasted_iota(jnp.int32, (length, span), 0)
        col = lax.broadcasted_iota(jnp.int32, (length, span), 1)
        distance = row - col + WINDOW
        allowed = (distance >= 0) & (distance < WINDOW) & ((col >= WINDOW) | (z > 0))
        kv = kvbuf[b]
        p = wqs[b]
        k, v = kv[:, :HEAD_DIM], kv[:, HEAD_DIM:]
        heads_out = []
        for j in range(heads):
            score = dot_t(p[:, j * HEAD_DIM:(j + 1) * HEAD_DIM], k) * HEAD_DIM ** -0.5
            score = jnp.where(allowed, score, -jnp.inf)
            sk = sink[0:1, j:j + 1]
            top_score = jnp.maximum(jnp.max(score, axis=1, keepdims=True), sk)
            e = jnp.exp(score - top_score)
            total = jnp.sum(e, axis=1, keepdims=True) + jnp.exp(sk - top_score)
            heads_out.append((dot(e.astype(bf16), v) / total).astype(bf16))
        rows[b, :, GLA_VALUE:] = jnp.concatenate(heads_out, axis=1)

    @pl.when(z == NZ - 1)
    def _():
        for b in range(NF):
            state_copy(b).wait_recv()

    @pl.loop(0, NF)
    def _(b):
        oacc[b] = oacc[b] + dot(reach[b], state_in[b])

    arrive(2)
    gate = project(W3, 0, GLA_VALUE).astype(f32)
    o = oacc[...]
    scaled = o * lax.rsqrt(jnp.mean(o * o, axis=2, keepdims=True) + norm_epsilon)
    rows[:, :, :GLA_VALUE] = (scaled * gain[...] * (gate / (1.0 + jnp.exp(-gate)))).astype(bf16)

    A, B = slice(0, half), slice(half, length)
    part_copies = [
        remote(part.at[0, top], dA, psend.at[0], precv.at[0], "fs", fx),
        remote(part.at[0, low_half], dB, psend.at[1], precv.at[1], "fs", fy),
        remote(part.at[1, top], rx.at[top], psend.at[2], precv.at[2], "fs", fx),
        remote(part.at[2, low_half], ry.at[low_half], psend.at[3], precv.at[3], "fs", fy),
        remote(part.at[1, low_half], rx.at[low_half], psend.at[4], precv.at[4], "fs", fx),
        remote(part.at[2, top], ry.at[top], psend.at[5], precv.at[5], "fs", fy),
    ]
    part[0] = dot(rows[fd], out_w[...]).astype(bf16)
    part_copies[0].start()
    part_copies[1].start()
    part[1, A] = dot(rows[fx, A], out_w[...]).astype(bf16)
    part_copies[2].start()
    part[2, B] = dot(rows[fy, B], out_w[...]).astype(bf16)
    part_copies[3].start()
    yx = dot(rows[fx, B], out_w[...])
    part_copies[1].wait_recv()
    part[1, B] = (yx + dB[...].astype(f32)).astype(bf16)
    part_copies[4].start()
    yy = dot(rows[fy, A], out_w[...])
    part_copies[0].wait_recv()
    part[2, A] = (yy + dA[...].astype(f32)).astype(bf16)
    part_copies[5].start()
    acc = dot(rows[f], out_w[...])
    for n in (2, 3):
        part_copies[n].wait_recv()
    for n in (4, 5):
        part_copies[n].wait_recv()
    out[0] = (acc + rx[...].astype(f32) + ry[...].astype(f32)).astype(bf16)

    for c in part_copies:
        c.wait_send()
    for n in range(6):
        token_copy(n).wait_send()
    for n in range(len(pieces)):
        for d in range(1, NZ):
            weight_copy(n, d).wait_send()
        for e in range(1, NT):
            own_copy(n, e).wait_send()
    for g in range(3):
        for d in range(1, NZ):
            for e in range(1, NT):
                forward_copy(g, d, e).wait_send()

    @pl.when(z < NZ - 1)
    def _():
        halo_copy().wait_send()
        for b in range(NF):
            state_copy(b).wait_send()


def shards(
    NZ, NF, NT,
    tokens, linear_query, linear_key, linear_decay, linear_value, linear_gate, decay_bias,
    norm_gain, window_query, window_key, window_value, sink_logit, linear_output, window_output,
):
    _, length, depth = tokens.shape
    assert NF == 4 and length >= WINDOW
    window_kv = jnp.concatenate([window_key, window_value], axis=1)
    groups = (
        (linear_decay, linear_key, linear_query, linear_value),
        (window_query, window_kv),
        (linear_gate,),
    )
    places, widths = [], []
    for group in groups:
        col, cols = 0, []
        for w in group:
            cols.append(col)
            col += w.shape[1]
        places.append(tuple(cols))
        widths.append(col)
    kb = linear_query.shape[0]
    n = NZ * NT
    levels = []
    h = 1
    while h < length:
        levels.append(h)
        h *= 2
    vm = pltpu.VMEM
    dma = pltpu.SemaphoreType.DMA
    kv_width = window_kv.shape[1]
    out_rows = linear_output.shape[0] + window_output.shape[0]
    anyspec, vspec = pl.BlockSpec(memory_space=pl.ANY), pl.BlockSpec(memory_space=vm)
    return pl.pallas_call(
        functools.partial(kernel, NZ, NF, NT, tuple(levels), tuple(places)),
        out_shape=jax.ShapeDtypeStruct((1, length, depth), bf16),
        in_specs=[anyspec] * 8 + [vspec] * 3 + [anyspec] * 2,
        out_specs=vspec,
        scratch_shapes=[
            vm((NF, length, depth), bf16),
            vm((n, kb, widths[0]), bf16),
            vm((n, kb, widths[1]), bf16),
            vm((n, kb, widths[2]), bf16),
            vm((out_rows, depth), bf16),
            vm((len(levels) + 2, length, length), bf16),
            vm((NF, length, GLA_KEY), bf16),
            vm((NF, length, GLA_KEY), bf16),
            vm((NF, length, GLA_KEY), bf16),
            vm((NF, length, GLA_VALUE), bf16),
            vm((NF, length + WINDOW, kv_width), bf16),
            vm((NF, length, GLA_KEY), bf16),
            vm((NF, length, window_query.shape[1]), bf16),
            vm((NF, length, GLA_KEY), bf16),
            vm((NF, length, GLA_VALUE), f32),
            vm((NF, GLA_KEY, GLA_VALUE), f32),
            vm((NF, GLA_KEY, GLA_VALUE), f32),
            vm((NF, GLA_KEY, GLA_VALUE), bf16),
            vm((NF, GLA_KEY, GLA_VALUE), bf16),
            vm((NF, length, out_rows), bf16),
            vm((3, length, depth), bf16),
            vm((length, depth), bf16),
            vm((length, depth), bf16),
            vm((length // 2, depth), bf16),
            vm((length // 2, depth), bf16),
            dma((10,)),
            dma((7, NZ)), dma((7, NZ)),
            dma((7, NT)), dma((7, NT)),
            dma((3, NZ, NT)), dma((3, NZ, NT)),
            dma((6,)), dma((6,)),
            dma((NF,)), dma((NF,)),
            dma, dma,
            dma((6,)), dma((6,)),
        ],
        compiler_params=pltpu.CompilerParams(
            collective_id=0, has_side_effects=True, vmem_limit_bytes=60 * 1024 * 1024),
        name="layer",
    )(tokens, linear_decay, linear_key, linear_query, linear_value, window_query, window_kv, linear_gate,
      decay_bias[None], norm_gain[None], sink_logit[None], linear_output, window_output)


def solution(mesh):
    shape = mesh.shape
    return jax.shard_map(
        functools.partial(shards, shape["sp"], shape["fs"], shape["tp"]),
        mesh=mesh,
        in_specs=(
            P(("fs", "tp"), "sp", None),
            P(("sp", "tp"), "fs"),
            P(("sp", "tp"), "fs"),
            P(("sp", "tp"), "fs"),
            P(("sp", "tp"), "fs"),
            P(("sp", "tp"), "fs"),
            P("fs"),
            P(),
            P(("sp", "tp"), "fs"),
            P(("sp", "tp"), "fs"),
            P(("sp", "tp"), "fs"),
            P("fs"),
            P("fs", None),
            P("fs", None),
        ),
        out_specs=P(("fs", "tp"), "sp", None),
        check_vma=False,
    )
```

time: 146 us -> 123 us (0.84)
  Pallas kernels: 134 us -> 119 us
  other arithmetic: 4.78 us -> 0.73 us
  local copies, waits for them, and re-layouts: 5.65 us -> 3.08 us
    pallas_call x1, Pallas kernels: 134 us -> 119 us  [shards(): pl.pallas_call(functools.partial(kernel, NZ, NF, NT, tuple(levels), tuple...]
    concatenate x2 -> x1, other arithmetic: 4.78 us -> 0.73 us  [shards(): window_kv = jnp.concatenate([window_key, window_value], axis=1)]
    concatenate x1 -> x0, local copies, waits for them, and re-layouts: 1.81 us -> none  [shards(): jnp.concatenate([linear_decay, linear_key, linear_value, window_key, wind...]
    unnamed x3 -> x5, local copies, waits for them, and re-layouts: 3.83 us -> 3.08 us
where the time goes in v2:
time: 123 us
  Pallas kernels  119 us (97%)
  local copies, waits for them, and re-layouts  3.08 us (3%)
    pallas_call x1, Pallas kernels, shards(): pl.pallas_call(functools.partial(kernel, NZ, NF, NT, tuple(levels), tuple...  119 us
    unnamed x5, local copies, waits for them, and re-layouts  3.08 us

profile of v2, /device:TPU:24, one launch (start us, length us, event | category | flops | bytes accessed | tf_op | source)
XLA Modules:
  0.0 122.7 jit_solution(3500097001302593284)
XLA Ops:
  0.0 0.0 copy-start
  0.0 0.9 copy.15
  0.9 0.0 copy-done
  0.9 0.1 copy.16
  1.0 0.7 pad_maximum_fusion.wkv_w
  1.7 118.8 %layer.1 = bf16[1,192,2048]{2,1,0:T(8,128)(2,1)} custom-call(bf16[1,192,2048]{2,1,0:T(8,128)(2,1)} %tok.1, bf16[256,128]{1,0:T(8,128)(2,1)} %decay_w.1, bf16[256,128]{1,0:T(8,128)(2,1)} %key_w.1, bf16[256,128]{1,0:T(8,128)(2,1)} %query_w.1, bf16[256,256]{1,0:T(8,128)(2,1)} %value_w.1, bf16[256,256]{1,0:T(8,128)(2,1)} %wquery_w.1, ...), custom_call_target="tpu_custom_call" | custom-call | tf_op jit(solution)/shard_map/layer/pallas_call | solution.py:352
  120.6 2.1 %copy.18 = bf16[1,192,2048]{2,1,0:T(8,128)(2,1)} copy(bf16[1,192,2048]{2,1,0:T(8,128)(2,1)} %layer.1) | data formatting | bytes 1572864
Async XLA Ops:
  0.0 0.9 copy-start

commit v3 on v2

--- a/solution.py
+++ b/solution.py
@@ -33,7 +33,7 @@
     NZ, NF, NT, levels, places,
     tok, decay_w, key_w, query_w, value_w, wquery_w, wkv_w, gate_w, bias, gain, sink, lin_w, win_w,
     out,
-    toks, W1, W2, W3, out_w, sums, fhi, flo, kkey, val, kvbuf, qs, wqs, reach, oacc, loc_state, loc_decay,
+    toks, W1, W2, W3, out_w, sums, fboth, kkey, val, kvbuf, qs, wqs, reach, oacc, loc_state, loc_decay,
     state_in, state_out, rows, part, rx, ry, dA, dB,
     loc_sem, wsend, wrecv, osend, orecv, fsend, frecv, tsend, trecv, ssend, srecv, hsend, hrecv, psend, precv,
 ):
@@ -145,8 +145,8 @@
                 forward_copy(g, d, e).wait_recv()
 
     def log_sum(n, b):
-        m = sums[n]
-        return dot(m, fhi[b]) + dot(m, flo[b])
+        both = dot(sums[n], fboth[b])
+        return both[:, :GLA_KEY] + both[:, GLA_KEY:]
 
     def project(buffer, col, width):
         x = toks[...].reshape(NF * length, depth)
@@ -160,8 +160,8 @@
     x = pair[:, :, :GLA_KEY].astype(f32) + bias[...]
     forget = (jnp.minimum(x, 0.0) - jnp.log1p(jnp.exp(-jnp.abs(x)))) / tau
     hi = forget.astype(bf16)
-    fhi[...] = hi
-    flo[...] = (forget - hi.astype(f32)).astype(bf16)
+    fboth[:, :, :GLA_KEY] = hi
+    fboth[:, :, GLA_KEY:] = (forget - hi.astype(f32)).astype(bf16)
     kkey[...] = pair[:, :, GLA_KEY:]
     rest = project(W1, 2 * GLA_KEY, GLA_KEY + GLA_VALUE)
     qs[...] = rest[:, :, :GLA_KEY]
@@ -181,15 +181,21 @@
         state = dot_rows(faded, val[b])
         ones = jnp.ones((length, GLA_VALUE), bf16)
         loc_state[b] = state
-        loc_decay[b] = jnp.exp(dot_rows(fhi[b], ones) + dot_rows(flo[b], ones))
+        loc_decay[b] = jnp.exp(dot_rows(fboth[b, :, :GLA_KEY], ones) + dot_rows(fboth[b, :, GLA_KEY:], ones))
 
         @pl.when(z == 0)
         def _():
             state_out[b] = state.astype(bf16)
             state_copy(b).start()
 
-    @pl.loop(0, NF)
-    def _(b):
+    def pass_state(b):
+        @pl.when((z > 0) & (z < NZ - 1))
+        def _():
+            state_copy(b).wait_recv()
+            state_out[b] = (state_in[b].astype(f32) * loc_decay[b] + loc_state[b]).astype(bf16)
+            state_copy(b).start()
+
+    def inside(b):
         q = qs[b].astype(f32) * GLA_KEY ** -0.5
         k = kkey[b].astype(f32)
         ri = lax.broadcasted_iota(jnp.int32, (length, length), 0)
@@ -204,13 +210,15 @@
             same = (ri & ~(2 * h - 1)) == (ci & ~(2 * h - 1))
             scores = scores + jnp.where(same, dot_t(qh, kh), 0.0)
         reach[b] = (q * jnp.exp(log_sum(len(levels), b))).astype(bf16)
-        oacc[b] = dot(scores.astype(bf16), val[b])
-
-        @pl.when((z > 0) & (z < NZ - 1))
-        def _():
-            state_copy(b).wait_recv()
-            state_out[b] = (state_in[b].astype(f32) * loc_decay[b] + loc_state[b]).astype(bf16)
-            state_copy(b).start()
+        return dot(scores.astype(bf16), val[b])
+
+    @pl.loop(0, NF // 2)
+    def _(pair_id):
+        first, second = inside(2 * pair_id), inside(2 * pair_id + 1)
+        oacc[2 * pair_id] = first
+        oacc[2 * pair_id + 1] = second
+        for b in (2 * pair_id, 2 * pair_id + 1):
+            pass_state(b)
 
     arrive(1)
     heads = sink.shape[1]
@@ -229,8 +237,7 @@
 
     span = length + WINDOW
 
-    @pl.loop(0, NF)
-    def _(b):
+    def window(b):
         row = lax.broadcasted_iota(jnp.int32, (length, span), 0)
         col = lax.broadcasted_iota(jnp.int32, (length, span), 1)
         distance = row - col + WINDOW
@@ -247,7 +254,13 @@
             e = jnp.exp(score - top_score)
             total = jnp.sum(e, axis=1, keepdims=True) + jnp.exp(sk - top_score)
             heads_out.append((dot(e.astype(bf16), v) / total).astype(bf16))
-        rows[b, :, GLA_VALUE:] = jnp.concatenate(heads_out, axis=1)
+        return jnp.concatenate(heads_out, axis=1)
+
+    @pl.loop(0, NF // 2)
+    def _(pair_id):
+        first, second = window(2 * pair_id), window(2 * pair_id + 1)
+        rows[2 * pair_id, :, GLA_VALUE:] = first
+        rows[2 * pair_id + 1, :, GLA_VALUE:] = second
 
     @pl.when(z == NZ - 1)
     def _():
@@ -361,8 +374,7 @@
             vm((n, kb, widths[2]), bf16),
             vm((out_rows, depth), bf16),
             vm((len(levels) + 2, length, length), bf16),
-            vm((NF, length, GLA_KEY), bf16),
-            vm((NF, length, GLA_KEY), bf16),
+            vm((NF, length, 2 * GLA_KEY), bf16),
             vm((NF, length, GLA_KEY), bf16),
             vm((NF, length, GLA_VALUE), bf16),
             vm((NF, length + WINDOW, kv_width), bf16),

time: 123 us -> 120 us (0.976)
  Pallas kernels: 119 us -> 116 us
    pallas_call x1, Pallas kernels: 119 us -> 116 us  [shards(): pl.pallas_call(functools.partial(kernel, NZ, NF, NT, tuple(levels), tuple...]
where the time goes in v3:
time: 120 us; the launch traced here: 119 us
  Pallas kernels  116 us (97%)
  local copies, waits for them, and re-layouts  3.08 us (3%)
    pallas_call x1, Pallas kernels, shards(): pl.pallas_call(functools.partial(kernel, NZ, NF, NT, tuple(levels), tuple...  116 us
    unnamed x5, local copies, waits for them, and re-layouts  3.08 us

profile of v3, /device:TPU:24, one launch (start us, length us, event | category | flops | bytes accessed | tf_op | source)
XLA Modules:
  0.0 119.5 jit_solution(4645536584450415994)
XLA Ops:
  0.0 0.0 copy-start
  0.0 0.9 copy.15
  0.9 0.0 copy-done
  0.9 0.1 copy.16
  1.0 0.7 pad_maximum_fusion.wkv_w
  1.7 115.6 %layer.1 = bf16[1,192,2048]{2,1,0:T(8,128)(2,1)} custom-call(bf16[1,192,2048]{2,1,0:T(8,128)(2,1)} %tok.1, bf16[256,128]{1,0:T(8,128)(2,1)} %decay_w.1, bf16[256,128]{1,0:T(8,128)(2,1)} %key_w.1, bf16[256,128]{1,0:T(8,128)(2,1)} %query_w.1, bf16[256,256]{1,0:T(8,128)(2,1)} %value_w.1, bf16[256,256]{1,0:T(8,128)(2,1)} %wquery_w.1, ...), custom_call_target="tpu_custom_call" | custom-call | tf_op jit(solution)/shard_map/layer/pallas_call | solution.py:365
  117.4 2.1 %copy.18 = bf16[1,192,2048]{2,1,0:T(8,128)(2,1)} copy(bf16[1,192,2048]{2,1,0:T(8,128)(2,1)} %layer.1) | data formatting | bytes 1572864
Async XLA Ops:
  0.0 0.9 copy-start
